TPU v7x, 32 devices: a whole 2x2x4 slice. The times are simulated.
32 devices in a mesh: rep: 2 (over x), fs: 8 (over z, y), tp: 2 (over core).
Axes of the slice: x: 2, y: 2, z: 4, core: 2. Of those that a mesh axis runs over, the one named last changes fastest.
Arguments:
- tokens: bfloat16 [6144, 2048], P(('rep', 'fs', 'tp')), may hold values from -6 to 6
- mix_gain_in: float32 [2048], replicated, may hold values from 0.1 to 1.9
- pool_weight: bfloat16 [4, 512, 512], P(None, 'fs'), may hold values from -0.25 to 0.25
- mix_gain_out: float32 [2048], replicated, may hold values from 0.1 to 1.9
- ffn_gain_in: float32 [2048], replicated, may hold values from 0.1 to 1.9
- gate_weight: bfloat16 [2048, 5632], P('fs', 'tp'), may hold values from -0.125 to 0.125
- up_weight: bfloat16 [2048, 5632], P('fs', 'tp'), may hold values from -0.125 to 0.125
- gate_taps: float32 [3, 5632], replicated, may hold values from -3.5 to 3.5
- up_taps: float32 [3, 5632], replicated, may hold values from -3.5 to 3.5
- down_weight: bfloat16 [5632, 2048], P('tp', 'fs'), may hold values from -0.078125 to 0.078125
- ffn_gain_out: float32 [2048], replicated, may hold values from 0.1 to 1.9
Outputs:
- mixed_out: bfloat16 [6144, 2048], P(('rep', 'fs', 'tp'))
All inputs are finite; a program needn't handle non-finite values.
Results may differ from a plain program's by a relative error of at most 0.014.
Values may be sent and summed in bfloat16 or wider, within the bound.
A program may use at most 128 MiB of HBM per device.

v0:
```python
import jax
import jax.numpy as jnp
from jax import lax
from jax.sharding import PartitionSpec as P

pool_spans = (2, 4, 8, 16)
rms_eps = 1e-06


def rms_scale(values, gain):
    floats = values.astype(jnp.float32)
    return floats * lax.rsqrt(jnp.mean(floats * floats, axis=-1, keepdims=True) + rms_eps) * gain


def pooled_gap(padded, count):
    margin = padded.shape[0] - count
    floats = padded.astype(jnp.float32)
    width = padded.shape[1] // len(pool_spans)
    where = jnp.arange(count, dtype=jnp.int32)
    pieces = []
    for group, span in enumerate(pool_spans):
        block = floats[:, group * width : (group + 1) * width]
        total = jnp.zeros((count, width), jnp.float32)
        for back in range(span):
            total = total + block[margin - back : margin - back + count]
        divisor = jnp.minimum(where + 1, span).astype(jnp.float32)
        pieces.append(total / divisor[:, None] - block[margin:])
    return jnp.concatenate(pieces, axis=1).astype(jnp.bfloat16)


def mix_groups(gap, pool_full):
    length, features = gap.shape
    groups = pool_full.shape[0]
    shaped = gap.reshape(length, groups, features // groups)
    result = jnp.einsum("rgc,gcj->rgj", shaped, pool_full, preferred_element_type=jnp.float32)
    return result.reshape(length, features).astype(jnp.bfloat16)


def causal_taps(pre, taps):
    width = taps.shape[0]
    floats = pre.astype(jnp.float32)
    padded = jnp.concatenate([jnp.zeros((width - 1, pre.shape[1]), jnp.float32), floats], axis=0)
    total = jnp.zeros(floats.shape, jnp.float32)
    for offset in range(width):
        total = total + taps[offset] * padded[offset : offset + pre.shape[0]]
    return total


def shards(
    tokens,
    mix_gain_in,
    pool_weight,
    mix_gain_out,
    ffn_gain_in,
    gate_weight,
    up_weight,
    gate_taps,
    up_taps,
    down_weight,
    ffn_gain_out,
):
    rows, features = tokens.shape
    margin = max(pool_spans) - 1
    position = lax.axis_index("tp")
    pool_full = lax.all_gather(pool_weight, "fs", axis=1, tiled=True)
    every = lax.all_gather(tokens, "tp", axis=0, tiled=True)
    length = every.shape[0]
    normed = rms_scale(every, mix_gain_in).astype(jnp.bfloat16)
    padded = jnp.concatenate([jnp.zeros((margin, features), jnp.bfloat16), normed], axis=0)
    gap = pooled_gap(padded, length)
    mixed = mix_groups(gap, pool_full)
    after_all = every.astype(jnp.float32) + rms_scale(mixed, mix_gain_out)
    whole = rms_scale(after_all, ffn_gain_in).astype(jnp.bfloat16)
    after_mix = lax.dynamic_slice_in_dim(after_all, position * rows, rows, 0)
    columns = gate_weight.shape[1]
    gate_part = jnp.dot(
        whole,
        lax.all_gather(gate_weight, "fs", axis=0, tiled=True),
        preferred_element_type=jnp.float32,
    )
    up_part = jnp.dot(
        whole,
        lax.all_gather(up_weight, "fs", axis=0, tiled=True),
        preferred_element_type=jnp.float32,
    )
    offset = position * columns
    gate_local = lax.dynamic_slice_in_dim(gate_taps, offset, columns, 1)
    up_local = lax.dynamic_slice_in_dim(up_taps, offset, columns, 1)
    gate_conv = causal_taps(gate_part.astype(jnp.bfloat16), gate_local)
    up_conv = causal_taps(up_part.astype(jnp.bfloat16), up_local)
    hidden = (jax.nn.gelu(gate_conv, approximate=True) * up_conv).astype(jnp.bfloat16)
    down_full = lax.all_gather(down_weight, "fs", axis=1, tiled=True)
    channel_out = lax.psum_scatter(
        jnp.dot(hidden, down_full, preferred_element_type=jnp.float32).astype(jnp.bfloat16),
        "tp",
        scatter_dimension=0,
        tiled=True,
    ).astype(jnp.float32)
    return (after_mix + rms_scale(channel_out, ffn_gain_out)).astype(jnp.bfloat16)


def solution(mesh):
    in_specs = (
        P(("rep", "fs", "tp"), None),
        P(),
        P(None, "fs", None),
        P(),
        P(),
        P("fs", "tp"),
        P("fs", "tp"),
        P(),
        P(),
        P("tp", "fs"),
        P(),
    )
    out_specs = P(("rep", "fs", "tp"), None)
    return jax.shard_map(shards, mesh=mesh, in_specs=in_specs, out_specs=out_specs, check_vma=False)
```

profile of v0, /device:TPU:0, one launch (start us, length us, event | category | flops | bytes accessed | tf_op | source)
XLA Modules:
  0.0 600.9 jit_solution(8342491924516857888)
XLA Ops:
  6.5 0.7 all-gather.6.cloned.1.call-update
  7.3 0.0 all-gather.8.cloned.1.call-start
  7.3 0.7 all-gather.8.cloned.1.call-update
  8.0 0.0 all-gather.10.cloned.1.call-start
  8.1 0.7 all-gather.10.cloned.1.call-update
  8.8 0.0 all-gather.12.cloned.1.call-start
  8.8 0.5 all-gather.12.cloned.1.call-update
  9.3 0.0 all-gather.14.cloned.1.call-start
  9.4 0.5 all-gather.14.cloned.1.call-update
  9.9 0.0 reduce-scatter.2.cloned.1.call-start
  10.0 1.2 dynamic-slice_reduce_fusion.2
  11.2 10.2 %all-gather.6.cloned.1.call-done = bf16[384,2048]{1,0:T(8,128)(2,1)} async-done(((bf16[192,2048]{1,0:T(8,128)(2,1)}), bf16[384,2048]{1,0:T(8,128)(2,1)}) %all-gather.6.cloned.1.call-update) | async-done | bytes 1572880 | tf_op jit(solution)/shard_map/all_gather | solution.py:66
  21.4 1.8 fusion.12
  23.2 1.8 fusion.14
  25.1 0.5 pad_convert_fusion
  25.5 1.0 fusion.51
  26.5 1.2 fusion.48
  27.7 46.2 %all-gather.8.cloned.1.call-done = bf16[4,512,512]{2,1,0:T(8,128)(2,1)} async-done(((bf16[4,64,512]{2,1,0:T(8,128)(2,1)}), bf16[4,512,512]{2,1,0:T(8,128)(2,1)}) %all-gather.8.cloned.1.call-update) | async-done | bytes 2097168 | tf_op jit(solution)/shard_map/all_gather | solution.py:65
  73.9 2.7 fusion.11
  76.6 0.4 convert_bitcast_fusion
  77.0 0.3 copy.13
  77.3 1.1 copy-done
  78.4 0.8 multiply_reduce_fusion
  79.2 158.8 %all-gather.10.cloned.1.call-done = bf16[2048,2816]{1,0:T(8,128)(2,1)} async-done(((bf16[256,2816]{1,0:T(8,128)(2,1)}), bf16[2048,2816]{1,0:T(8,128)(2,1)}) %all-gather.10.cloned.1.call-update) | async-done | bytes 11534352 | tf_op jit(solution)/shard_map/all_gather | solution.py:78
  238.0 9.7 %fusion.10 = f32[384,2816]{1,0:T(8,128)} fusion(bf16[2048,2816]{1,0:T(8,128)(2,1)} %all-gather.10.cloned.1.call-done, f32[384,2048]{1,0:T(8,128)S(1)} %get-tuple-element.12, f32[2048]{0:T(1024)S(1)} %copy-done.4, f32[384]{0:T(512)S(1)} %add_rsqrt_fusion), kind=kOutput, calls=%fused_computation.16 | convolution fusion | flops 4433707008 | bytes 19015168 | tf_op jit(solution)/shard_map/dot_general | solution.py:76
  247.6 153.9 %all-gather.12.cloned.1.call-done = bf16[2048,2816]{1,0:T(8,128)(2,1)} async-done(((bf16[256,2816]{1,0:T(8,128)(2,1)}), bf16[2048,2816]{1,0:T(8,128)(2,1)}) %all-gather.12.cloned.1.call-update) | async-done | bytes 11534352 | tf_op jit(solution)/shard_map/all_gather | solution.py:83
  401.5 9.6 %fusion.9 = f32[384,2816]{1,0:T(8,128)} fusion(bf16[2048,2816]{1,0:T(8,128)(2,1)} %all-gather.12.cloned.1.call-done, f32[384,2048]{1,0:T(8,128)S(1)} %get-tuple-element.12, f32[2048]{0:T(1024)S(1)} %copy-done.4, f32[384]{0:T(512)S(1)} %add_rsqrt_fusion), kind=kOutput, calls=%fused_computation.14 | convolution fusion | flops 4433707008 | bytes 19015168 | tf_op jit(solution)/shard_map/dot_general | solution.py:81
  411.1 153.8 %all-gather.14.cloned.1.call-done = bf16[2816,2048]{1,0:T(8,128)(2,1)} async-done(((bf16[2816,256]{1,0:T(8,128)(2,1)}), bf16[2816,2048]{1,0:T(8,128)(2,1)}) %all-gather.14.cloned.1.call-update) | async-done | bytes 11534352 | tf_op jit(solution)/shard_map/all_gather | solution.py:92
  565.0 18.0 %convolution_convert_fusion.2 = bf16[384,2048]{1,0:T(8,128)(2,1)} fusion(bf16[2816,2048]{1,0:T(8,128)(2,1)} %all-gather.14.cloned.1.call-done, f32[384,2816]{1,0:T(8,128)} %fusion.9, f32[384,2816]{1,0:T(8,128)} %fusion.10, f32[2816]{0:T(1024)S(1)} %get-tuple-element.10, f32[2816]{0:T(1024)S(1)} %get-tuple-element.9, f32[2816]{0:T(1024)S(1)} %get-tuple-element.8, ...), kind=kOutput, calls=%fused_computation.25 | convolution fusion | flops 4451598336 | bytes 21825536 | tf_op jit(solution)/shard_map/dot_general | solution.py:94
  583.0 7.4 %reduce-scatter.2.cloned.1.call-done = bf16[192,2048]{1,0:T(8,128)(2,1)} async-done(((bf16[384,2048]{1,0:T(8,128)(2,1)}), bf16[192,2048]{1,0:T(8,128)(2,1)}) %reduce-scatter.2.cloned.1.call-update) | async-done | bytes 786448 | tf_op jit(solution)/shard_map/reduce_scatter | solution.py:93
  590.3 1.4 fusion.25
  591.7 2.3 fusion.28
  (18 shorter events, 0.1 us)
Async XLA Ops:
  6.5 14.9 %all-gather.6.cloned.1.call-start = ((), (), s32[]{:S(2)}) async-start(), calls=%async_computation.1 | async-start | bytes 2359296 | tf_op jit(solution)/shard_map/all_gather | solution.py:66
  7.3 16.0 %copy-start.1 = (f32[2048]{0:T(1024)S(1)}, f32[2048]{0:T(1024)}, u32[]{:S(2)}) copy-start(f32[2048]{0:T(1024)} %param.12) | copy-start | bytes 24580
  7.3 66.6 %all-gather.8.cloned.1.call-start = ((), (), s32[]{:S(2)}) async-start(), calls=%async_computation.2 | async-start | bytes 2359296 | tf_op jit(solution)/shard_map/all_gather | solution.py:65
  8.0 229.9 %all-gather.10.cloned.1.call-start = ((), (), s32[]{:S(2)}) async-start(), calls=%async_computation.3 | async-start | bytes 12976128 | tf_op jit(solution)/shard_map/all_gather | solution.py:78
  8.8 392.8 %all-gather.12.cloned.1.call-start = ((), (), s32[]{:S(2)}) async-start(), calls=%async_computation.4 | async-start | bytes 12976128 | tf_op jit(solution)/shard_map/all_gather | solution.py:83
  9.3 555.6 %all-gather.14.cloned.1.call-start = ((), (), s32[]{:S(2)}) async-start(), calls=%async_computation.5 | async-start | bytes 12976128 | tf_op jit(solution)/shard_map/all_gather | solution.py:92
  9.9 580.4 %reduce-scatter.2.cloned.1.call-start = ((), (), s32[]{:S(2)}) async-start(), calls=%async_computation.6 | async-start | bytes 2359296 | tf_op jit(solution)/shard_map/reduce_scatter | solution.py:93
  77.0 1.4 copy-start
  77.0 1.4 copy-start.3
  78.4 159.6 %copy-start.4 = (f32[2048]{0:T(1024)S(1)}, f32[2048]{0:T(1024)}, u32[]{:S(2)}) copy-start(f32[2048]{0:T(1024)} %param.15) | copy-start | bytes 24580
  565.0 26.8 %copy-start.2 = (f32[2048]{0:T(1024)S(1)}, f32[2048]{0:T(1024)}, u32[]{:S(2)}) copy-start(f32[2048]{0:T(1024)} %param.21) | copy-start | bytes 24580
Sparse Core Ops, SparseCore 0:
  8.9 12.5 all-gather.5
  23.6 50.2 all-gather.7
  76.1 161.8 all-gather.9
  240.0 161.4 all-gather.11
  403.4 161.4 all-gather.13
  583.1 7.2 reduce-scatter.1
where the time goes:
time: 601 us
  waiting for transfers between devices  533 us (89%)
  matrix products  39.9 us (7%)
  between operations  13.6 us (2%)
  other arithmetic  11.2 us (2%)
    all_gather x1, waiting for transfers between devices, shards(): lax.all_gather(gate_weight, 'fs', axis=0, tiled=True)  159 us
    all_gather x1, waiting for transfers between devices, shards(): lax.all_gather(up_weight, 'fs', axis=0, tiled=True)  154 us
    all_gather x1, waiting for transfers between devices, shards(): down_full = lax.all_gather(down_weight, 'fs', axis=1, tiled=True)  154 us
    all_gather x1, waiting for transfers between devices, shards(): pool_full = lax.all_gather(pool_weight, 'fs', axis=1, tiled=True)  46.2 us
    dot_general x1, matrix products, shards(): jnp.dot(hidden, down_full, preferred_element_type=jnp.float32)  18 us
  transfers between devices with their start and end apart: 6, of which 6 were waited for; matrix products, arithmetic and copies ran while one was open for 5% of the time, Pallas kernels for 0%

commit v1 on v0

--- a/solution.py
+++ b/solution.py
@@ -89,7 +89,12 @@
     gate_conv = causal_taps(gate_part.astype(jnp.bfloat16), gate_local)
     up_conv = causal_taps(up_part.astype(jnp.bfloat16), up_local)
     hidden = (jax.nn.gelu(gate_conv, approximate=True) * up_conv).astype(jnp.bfloat16)
-    down_full = lax.all_gather(down_weight, "fs", axis=1, tiled=True)
+
+    def _drive_slices(patch):
+        spare = lax.all_gather(patch, axis_name="fs")
+        return jnp.concatenate(spare, 1)
+
+    down_full = _drive_slices(down_weight)
     channel_out = lax.psum_scatter(
         jnp.dot(hidden, down_full, preferred_element_type=jnp.float32).astype(jnp.bfloat16),
         "tp",

time: 601 us -> 611 us (1.017)
  local copies, waits for them, and re-layouts: 2.58 us -> 18 us
    reshape x0 -> x1, local copies, waits for them, and re-layouts: none -> 15.4 us  [_drive_slices(): return jnp.concatenate(spare, 1)]
  transfers between devices with their start and end apart: 6 -> 6, of which waited for: 6 -> 6; matrix products, arithmetic and copies ran while one was open for 5% -> 6% of each run, Pallas kernels for 0% -> 0%
where the time goes in v1:
time: 611 us; the launch traced here: 610 us
  waiting for transfers between devices  528 us (86%)
  matrix products  39.7 us (6%)
  local copies, waits for them, and re-layouts  18 us (3%)
  between operations  13.6 us (2%)
  other arithmetic  11.2 us (2%)
    all_gather x1, waiting for transfers between devices, _drive_slices(): spare = lax.all_gather(patch, axis_name='fs')  159 us
    all_gather x1, waiting for transfers between devices, shards(): lax.all_gather(gate_weight, 'fs', axis=0, tiled=True)  154 us
    all_gather x1, waiting for transfers between devices, shards(): lax.all_gather(up_weight, 'fs', axis=0, tiled=True)  148 us
    all_gather x1, waiting for transfers between devices, shards(): pool_full = lax.all_gather(pool_weight, 'fs', axis=1, tiled=True)  46.2 us
    dot_general x1, matrix products, shards(): jnp.dot(hidden, down_full, preferred_element_type=jnp.float32)  17.7 us
    reshape x1, local copies, waits for them, and re-layouts, _drive_slices(): return jnp.concatenate(spare, 1)  15.4 us
  transfers between devices with their start and end apart: 6, of which 6 were waited for; matrix products, arithmetic and copies ran while one was open for 6% of the time, Pallas kernels for 0%

profile of v1, /device:TPU:0, one launch (start us, length us, event | category | flops | bytes accessed | tf_op | source)
XLA Modules:
  0.0 610.4 jit_solution(12383845677126318486)
XLA Ops:
  6.5 0.7 all-gather.7.cloned.1.call-update
  7.3 0.7 all-gather.9.cloned.1.call-update
  8.0 0.0 all-gather.15.cloned.1.call-start
  8.1 0.7 all-gather.15.cloned.1.call-update
  8.8 0.0 all-gather.13.cloned.1.call-start
  8.8 0.5 all-gather.13.cloned.1.call-update
  9.3 0.0 all-gather.11.cloned.1.call-start
  9.4 0.5 all-gather.11.cloned.1.call-update
  9.9 0.0 reduce-scatter.2.cloned.1.call-start
  10.0 1.2 dynamic-slice_reduce_fusion.2
  11.2 10.2 %all-gather.7.cloned.1.call-done = bf16[384,2048]{1,0:T(8,128)(2,1)} async-done(((bf16[192,2048]{1,0:T(8,128)(2,1)}), bf16[384,2048]{1,0:T(8,128)(2,1)}) %all-gather.7.cloned.1.call-update) | async-done | bytes 1572880 | tf_op jit(solution)/shard_map/all_gather | solution.py:66
  21.4 1.8 fusion.12
  23.2 1.8 fusion.14
  25.1 0.5 pad_convert_fusion
  25.5 1.0 fusion.51
  26.5 1.2 fusion.48
  27.7 46.2 %all-gather.9.cloned.1.call-done = bf16[4,512,512]{2,1,0:T(8,128)(2,1)} async-done(((bf16[4,64,512]{2,1,0:T(8,128)(2,1)}), bf16[4,512,512]{2,1,0:T(8,128)(2,1)}) %all-gather.9.cloned.1.call-update) | async-done | bytes 2097168 | tf_op jit(solution)/shard_map/all_gather | solution.py:65
  73.9 2.7 fusion.11
  76.5 0.4 convert_bitcast_fusion
  77.0 0.3 copy.16
  77.3 1.1 copy-done
  78.4 0.8 multiply_reduce_fusion
  79.2 158.8 %all-gather.15.cloned.1.call-done = bf16[22528,256]{1,0:T(8,128)(2,1)} async-done(((bf16[2816,256]{1,0:T(8,128)(2,1)}), bf16[22528,256]{1,0:T(8,128)(2,1)}) %all-gather.15.cloned.1.call-update) | async-done | bytes 11534352 | tf_op jit(solution)/shard_map/all_gather | solution.py:94
  238.0 15.4 %copy.15 = bf16[2816,8,256]{0,2,1:T(8,128)(2,1)} copy(bf16[2816,8,256]{2,0,1:T(8,128)(2,1)} %bitcast.21) | data formatting | bytes 23068672 | tf_op jit(solution)/shard_map/reshape | solution.py:95
  253.4 148.2 %all-gather.13.cloned.1.call-done = bf16[2048,2816]{1,0:T(8,128)(2,1)} async-done(((bf16[256,2816]{1,0:T(8,128)(2,1)}), bf16[2048,2816]{1,0:T(8,128)(2,1)}) %all-gather.13.cloned.1.call-update) | async-done | bytes 11534352 | tf_op jit(solution)/shard_map/all_gather | solution.py:83
  401.5 9.7 %fusion.9 = f32[384,2816]{1,0:T(8,128)} fusion(bf16[2048,2816]{1,0:T(8,128)(2,1)} %all-gather.13.cloned.1.call-done, f32[384,2048]{1,0:T(8,128)S(1)} %get-tuple-element.12, f32[2048]{0:T(1024)S(1)} %copy-done.4, f32[384]{0:T(512)S(1)} %add_rsqrt_fusion), kind=kOutput, calls=%fused_computation.14 | convolution fusion | flops 4433707008 | bytes 19015168 | tf_op jit(solution)/shard_map/dot_general | solution.py:81
  411.2 153.9 %all-gather.11.cloned.1.call-done = bf16[2048,2816]{1,0:T(8,128)(2,1)} async-done(((bf16[256,2816]{1,0:T(8,128)(2,1)}), bf16[2048,2816]{1,0:T(8,128)(2,1)}) %all-gather.11.cloned.1.call-update) | async-done | bytes 11534352 | tf_op jit(solution)/shard_map/all_gather | solution.py:78
  565.1 9.7 %fusion.10 = f32[384,2816]{1,0:T(8,128)} fusion(bf16[2048,2816]{1,0:T(8,128)(2,1)} %all-gather.11.cloned.1.call-done, f32[384,2048]{1,0:T(8,128)S(1)} %get-tuple-element.12, f32[2048]{0:T(1024)S(1)} %copy-done.4, f32[384]{0:T(512)S(1)} %add_rsqrt_fusion), kind=kOutput, calls=%fused_computation.16 | convolution fusion | flops 4433707008 | bytes 19015168 | tf_op jit(solution)/shard_map/dot_general | solution.py:76
  574.8 17.7 %convolution_convert_fusion.2 = bf16[384,2048]{1,0:T(8,128)(2,1)} fusion(bf16[2816,2048]{0,1:T(8,128)(2,1)} %bitcast.22, f32[384,2816]{1,0:T(8,128)} %fusion.9, f32[384,2816]{1,0:T(8,128)} %fusion.10, f32[2816]{0:T(1024)S(1)} %get-tuple-element.10, f32[2816]{0:T(1024)S(1)} %get-tuple-element.9, f32[2816]{0:T(1024)S(1)} %get-tuple-element.8, ...), kind=kOutput, calls=%fused_computation.25 | convolution fusion | flops 4451598336 | bytes 21825536 | tf_op jit(solution)/shard_map/dot_general | solution.py:99
  592.5 7.4 %reduce-scatter.2.cloned.1.call-done = bf16[192,2048]{1,0:T(8,128)(2,1)} async-done(((bf16[384,2048]{1,0:T(8,128)(2,1)}), bf16[192,2048]{1,0:T(8,128)(2,1)}) %reduce-scatter.2.cloned.1.call-update) | async-done | bytes 786448 | tf_op jit(solution)/shard_map/reduce_scatter | solution.py:98
  599.9 1.4 fusion.25
  601.2 2.3 fusion.28
  (19 shorter events, 0.1 us)
Async XLA Ops:
  6.5 14.9 %all-gather.7.cloned.1.call-start = ((), (), s32[]{:S(2)}) async-start(), calls=%async_computation.1 | async-start | bytes 2359296 | tf_op jit(solution)/shard_map/all_gather | solution.py:66
  7.3 16.0 %copy-start.1 = (f32[2048]{0:T(1024)S(1)}, f32[2048]{0:T(1024)}, u32[]{:S(2)}) copy-start(f32[2048]{0:T(1024)} %param.12) | copy-start | bytes 24580
  7.3 66.6 %all-gather.9.cloned.1.call-start = ((), (), s32[]{:S(2)}) async-start(), calls=%async_computation.2 | async-start | bytes 2359296 | tf_op jit(solution)/shard_map/all_gather | solution.py:65
  8.0 229.9 %all-gather.15.cloned.1.call-start = ((), (), s32[]{:S(2)}) async-start(), calls=%async_computation.6 | async-start | bytes 12976128 | tf_op jit(solution)/shard_map/all_gather | solution.py:94
  8.8 392.8 %all-gather.13.cloned.1.call-start = ((), (), s32[]{:S(2)}) async-start(), calls=%async_computation.4 | async-start | bytes 12976128 | tf_op jit(solution)/shard_map/all_gather | solution.py:83
  9.3 555.8 %all-gather.11.cloned.1.call-start = ((), (), s32[]{:S(2)}) async-start(), calls=%async_computation.3 | async-start | bytes 12976128 | tf_op jit(solution)/shard_map/all_gather | solution.py:78
  9.9 589.9 %reduce-scatter.2.cloned.1.call-start = ((), (), s32[]{:S(2)}) async-start(), calls=%async_computation.5 | async-start | bytes 2359296 | tf_op jit(solution)/shard_map/reduce_scatter | solution.py:98
  77.0 1.4 copy-start
  77.0 1.4 copy-start.3
  238.0 163.6 %copy-start.4 = (f32[2048]{0:T(1024)S(1)}, f32[2048]{0:T(1024)}, u32[]{:S(2)}) copy-start(f32[2048]{0:T(1024)} %param.15) | copy-start | bytes 24580
  574.8 26.5 %copy-start.2 = (f32[2048]{0:T(1024)S(1)}, f32[2048]{0:T(1024)}, u32[]{:S(2)}) copy-start(f32[2048]{0:T(1024)} %param.21) | copy-start | bytes 24580
Sparse Core Ops, SparseCore 0:
  8.9 12.5 all-gather.6
  23.6 50.2 all-gather.8
  76.1 161.8 all-gather.14
  240.0 161.4 all-gather.12
  403.6 161.4 all-gather.10
  592.6 7.2 reduce-scatter.1
